TPU v7x, 512 devices: a 4x2x32 block of a 4x8x32 slice. The times are simulated.
512 devices in a mesh: grp: 2 (over y), sp: 32 (over z), tp: 8 (over x, core).
Axes of the slice: x: 4, y: 2, z: 32, core: 2. Of those that a mesh axis runs over, the one named last changes fastest.
The devices are a block of a 4x8x32 slice.
Arguments:
- prompt: bfloat16 [8, 6144, 2048], P('grp', 'sp'), parts along dimension 0, may hold values from -6 to 6
- w_key: bfloat16 [2048, 2048], P('sp', 'tp'), may hold values from -0.125 to 0.125
- w_value: bfloat16 [2048, 2048], P('sp', 'tp'), may hold values from -0.125 to 0.125
- query_new: bfloat16 [8, 2048], P('grp', 'tp'), parts along dimension 0, may hold values from -150 to 150
- key_new: bfloat16 [8, 2048], P('grp', 'tp'), parts along dimension 0, may hold values from -15 to 15
- value_new: bfloat16 [8, 2048], P('grp', 'tp'), parts along dimension 0, may hold values from -6 to 6
- mix_lambda: float32 [16], P('tp'), may hold values from 0.3 to 0.8
- head_gain: float32 [128], replicated, may hold values from 0.1 to 1.9
Outputs:
- key_cache: bfloat16 [64, 32, 24, 2048], P(('grp', 'sp'), None, None, 'tp'), parts along dimension 0
- value_cache: bfloat16 [64, 32, 24, 2048], P(('grp', 'sp'), None, None, 'tp'), parts along dimension 0
- first_read: bfloat16 [8, 2048], P('grp', 'tp'), parts along dimension 0
There are 2 independent parts, one for each index of `grp`. A program takes and returns all parts, laid end to end along the dimension named above; an argument that names none is the same for every part. Nothing has to cross between parts.
All inputs are finite; a program needn't handle non-finite values.
Results may differ from a plain program's by a relative error of at most 0.0065.
The roundings to bfloat16 on the way count: a program that leaves them out, or rounds other values in their place, can miss the bound.
Values may be sent and summed in bfloat16 or wider, within the bound.
No kernel may reach another device: no remote copies, remote signals or barrier semaphores. Data moves between devices by JAX's collectives and lax.ppermute only.
A program may use at most 64 MiB of HBM per device.

v0:
```python
import jax
import jax.numpy as jnp
from jax import lax
from jax.sharding import PartitionSpec as P

HALF = 64
VDIM = 128


def sent_together(arrays, axis, dim, along):
    both = jnp.concatenate(arrays, axis=along)
    result, at, finished = (lax.all_gather(both, axis, axis=dim, tiled=True), 0, [])
    for a in arrays:
        finished.append(lax.slice_in_dim(result, at, at + a.shape[along], axis=along))
        at += a.shape[along]
    return tuple(finished)


def copy_for_each(shard, axis):
    peers = lax.axis_size(axis)
    return lax.all_to_all(
        jnp.broadcast_to(shard[None], (peers, *shard.shape)), axis, 0, 0, tiled=True
    )


def collected_together(shard, axis):
    leaves = jax.tree.leaves(shard)
    order = sorted(range(len(leaves)), key=lambda k: -leaves[k].size)
    width = (1, *leaves[order[0]].shape)[-1]
    lines = [
        jnp.pad(leaves[k].reshape(-1), (0, -leaves[k].size % width)).reshape(-1, width)
        for k in order
    ]
    both, at, found = (copy_for_each(jnp.concatenate(lines), axis), 0, {})
    for k, line in zip(order, lines):
        section = both[:, at : at + len(line)].reshape(len(both), -1)
        found[k] = section[:, : leaves[k].size].reshape(-1, *leaves[k].shape)
        at += len(line)
    numbers = iter(range(len(leaves)))
    return jax.tree.map(lambda _: found[next(numbers)], shard)


def combined_pairwise(pieces, combine):
    while len(jax.tree.leaves(pieces)[0]) > 1:
        pieces = jax.vmap(combine)(
            *(jax.tree.map(lambda part: part[side::2], pieces) for side in (0, 1))
        )
    return jax.tree.map(lambda part: part[0], pieces)


def merged(shard, axis, combine):
    pieces = collected_together(shard, axis)
    return combined_pairwise(pieces, combine)


def of_everyone(shard, axis):
    return copy_for_each(shard, axis).sum(axis=0)


def project(rows, w_key, w_value):
    pieces = sent_together((w_key, w_value), "sp", 0, 1)
    keys = jnp.dot(rows, pieces[0], preferred_element_type=jnp.float32)
    values = jnp.dot(rows, pieces[1], preferred_element_type=jnp.float32)
    return (keys.astype(jnp.bfloat16), values.astype(jnp.bfloat16))


def score_maps(query, keys):
    count, span = (keys.shape[0], keys.shape[1])
    heads = query.shape[1] // (2 * HALF)
    q_parts = query.reshape(count, heads, 2, HALF)
    k_parts = keys.reshape(count, span, heads, 2, HALF)
    return jnp.einsum(
        "shmc,slhmc->shml", q_parts, k_parts, preferred_element_type=jnp.float32
    ) * HALF ** (-0.5)


def own_scores(query, fresh_key):
    count = query.shape[0]
    heads = query.shape[1] // (2 * HALF)
    q_parts = query.astype(jnp.float32).reshape(count, heads, 2, HALF)
    k_parts = fresh_key.astype(jnp.float32).reshape(count, heads, 2, HALF)
    return jnp.sum(q_parts * k_parts, axis=-1) * HALF ** (-0.5)


def finish(reads, head_gain):
    mean = jnp.mean(reads * reads, axis=-1, keepdims=True)
    normed = reads * lax.rsqrt(mean + 1e-06) * head_gain
    return normed.reshape(reads.shape[0], -1).astype(jnp.bfloat16)


def join_totals(first, second):
    top = jnp.maximum(first[0], second[0])
    return (top, first[1] * jnp.exp(first[0] - top) + second[1] * jnp.exp(second[0] - top))


def placed(part_rows, prompts, first, fill):
    base = jnp.full((prompts,) + part_rows.shape[1:], fill, jnp.float32)
    return lax.dynamic_update_slice_in_dim(base, part_rows, first, 0)


def cache_read(query_new, key_new, value_new, keys, values, mix_lambda, head_gain, first):
    count, span = (keys.shape[0], keys.shape[1])
    prompts = query_new.shape[0]
    heads = mix_lambda.shape[0]
    query = lax.dynamic_slice_in_dim(query_new, first, count, 0)
    scores = score_maps(query, keys)
    fresh_all = own_scores(query_new, key_new)
    fresh = lax.dynamic_slice_in_dim(fresh_all, first, count, 0)
    local_top = jnp.maximum(jnp.max(scores, axis=-1), fresh)
    local_total = jnp.sum(jnp.exp(scores - local_top[..., None]), axis=-1)
    top_all, cache_total = merged(
        (placed(local_top, prompts, first, -1e30), placed(local_total, prompts, first, 0.0)),
        "sp",
        join_totals,
    )
    own = jnp.exp(fresh_all - top_all)
    total_all = cache_total + own
    top = lax.dynamic_slice_in_dim(top_all, first, count, 0)
    total = lax.dynamic_slice_in_dim(total_all, first, count, 0)
    probs = jnp.exp(scores - top[..., None]) / total[..., None]
    mixed = (probs[:, :, 0] - mix_lambda[None, :, None] * probs[:, :, 1]).astype(jnp.bfloat16)
    value_parts = values.reshape(count, span, heads, VDIM)
    partial_value = jnp.einsum(
        "shl,slhv->shv", mixed, value_parts, preferred_element_type=jnp.float32
    )
    reads = of_everyone(placed(partial_value, prompts, first, 0.0), "sp")
    own_prob = own / total_all
    own_mixed = (own_prob[:, :, 0] - mix_lambda[None, :] * own_prob[:, :, 1]).astype(jnp.bfloat16)
    reads = reads + own_mixed.astype(jnp.float32)[..., None] * value_new.astype(
        jnp.float32
    ).reshape(prompts, heads, VDIM)
    return finish(reads, head_gain)


def block_read(
    query_new, key_new, value_new, key_cache, value_cache, mix_lambda, head_gain, spread
):
    blocks, sub = (key_cache.shape[1], key_cache.shape[2])
    first = lax.axis_index("sp") // spread
    keys = key_cache.reshape(1, blocks * sub, -1)
    values = value_cache.reshape(1, blocks * sub, -1)
    return cache_read(query_new, key_new, value_new, keys, values, mix_lambda, head_gain, first)


def body(prompt, w_key, w_value, query_new, key_new, value_new, mix_lambda, head_gain):
    count, piece, width = prompt.shape
    spread = lax.axis_size("sp") // count
    sub = piece // spread
    keys, values = project(prompt.reshape(count * piece, width), w_key, w_value)
    key_blocks = keys.reshape(count * spread, 1, sub, -1)
    value_blocks = values.reshape(count * spread, 1, sub, -1)
    key_cache, value_cache = (
        lax.all_to_all(key_blocks, "sp", split_axis=0, concat_axis=1, tiled=True),
        lax.all_to_all(value_blocks, "sp", split_axis=0, concat_axis=1, tiled=True),
    )
    first_read = block_read(
        query_new, key_new, value_new, key_cache, value_cache, mix_lambda, head_gain, spread
    )
    return (key_cache, value_cache, first_read)


def solution(mesh):
    placed = (
        P("grp", "sp", None),
        P("sp", "tp"),
        P("sp", "tp"),
        P("grp", "tp"),
        P("grp", "tp"),
        P("grp", "tp"),
        P("tp"),
        P(),
    )
    return jax.shard_map(
        body,
        mesh=mesh,
        in_specs=placed,
        out_specs=(
            P(("grp", "sp"), None, None, "tp"),
            P(("grp", "sp"), None, None, "tp"),
            P("grp", "tp"),
        ),
        check_vma=False,
    )
```

profile of v0, /device:TPU:34, one launch (start us, length us, event | category | flops | bytes accessed | tf_op | source)
XLA Modules:
  0.0 364.4 jit_solution(18418636442365662421)
XLA Ops:
  7.3 1.6 pad_maximum_fusion
  8.9 164.9 %all-gather.2.cloned.1.call-done = bf16[2048,512]{1,0:T(8,128)(2,1)} async-done(((bf16[64,512]{1,0:T(8,128)(2,1)}), bf16[2048,512]{1,0:T(8,128)(2,1)}) %all-gather.2.cloned.1.call-update) | async-done | bytes 2097168 | tf_op jit(solution)/shard_map/all_gather | solution.py:12
  173.8 2.3 fusion
  176.1 0.9 copy.102
  177.0 11.1 %all-to-all-start = ((bf16[32,1,24,256]{3,2,1,0:T(8,128)(2,1)}), bf16[32,1,24,256]{3,2,1,0:T(8,128)(2,1)S(1)}, u32[]{:S(2)}, u32[]{:S(2)}) async-start(bf16[32,1,24,256]{3,2,1,0:T(8,128)(2,1)} %bitcast.90), calls=%async_computation | async-start | bytes 786432 | tf_op jit(solution)/shard_map/all_to_all | solution.py:153
  188.1 3.0 fusion.1
  191.1 1.9 copy.104
  193.1 32.8 %all-to-all-done = bf16[32,1,24,256]{3,2,1,0:T(8,128)(2,1)S(1)} async-done(((bf16[32,1,24,256]{3,2,1,0:T(8,128)(2,1)}), bf16[32,1,24,256]{3,2,1,0:T(8,128)(2,1)S(1)}, u32[]{:S(2)}, u32[]{:S(2)}) %all-to-all-start) | async-done | bytes 393248 | tf_op jit(solution)/shard_map/all_to_all | solution.py:153
  225.8 5.4 %all-to-all-start.1 = ((bf16[32,1,24,256]{3,2,1,0:T(8,128)(2,1)}), bf16[32,1,24,256]{3,2,1,0:T(8,128)(2,1)}, u32[]{:S(2)}, u32[]{:S(2)}) async-start(bf16[32,1,24,256]{3,2,1,0:T(8,128)(2,1)} %bitcast.89), calls=%async_computation.1 | async-start | bytes 786432 | tf_op jit(solution)/shard_map/all_to_all | solution.py:154
  231.3 0.7 reshape.134
  232.1 0.1 reduce_sum.40
  232.2 0.1 copy.106
  232.3 0.6 broadcast_multiply_fusion
  232.8 1.2 reshape.123
  234.1 1.5 fusion.4
  235.5 0.7 fusion.21
  236.2 1.3 copy.107
  237.5 1.3 dynamic-slice_maximum_fusion
  238.9 1.3 copy.109
  240.2 1.3 copy.108
  241.5 0.6 broadcast.51
  242.1 1.3 dynamic_update_slice.11
  243.4 1.3 reshape.124
  244.8 1.4 exponential_reduce_fusion
  246.2 1.3 copy.110
  247.5 0.6 broadcast.53
  248.1 1.3 dynamic_update_slice.12
  249.4 1.3 reshape.125
  250.7 1.3 pad_maximum_fusion.1
  252.1 17.1 %all-to-all-done.1 = bf16[32,1,24,256]{3,2,1,0:T(8,128)(2,1)} async-done(((bf16[32,1,24,256]{3,2,1,0:T(8,128)(2,1)}), bf16[32,1,24,256]{3,2,1,0:T(8,128)(2,1)}, u32[]{:S(2)}, u32[]{:S(2)}) %all-to-all-start.1) | async-done | bytes 393248 | tf_op jit(solution)/shard_map/all_to_all | solution.py:154
  269.1 1.3 broadcast_in_dim.9
  270.4 5.3 %all-to-all-start.2 = ((f32[32,16,2]{1,2,0:T(2,128)}), f32[32,16,2]{1,2,0:T(2,128)}, u32[]{:S(2)}, u32[]{:S(2)}) async-start(f32[32,16,2]{1,2,0:T(2,128)} %broadcast_in_dim.9), calls=%async_computation.2 | async-start | bytes 65536 | tf_op jit(solution)/shard_map/all_to_all | solution.py:21
  275.8 1.8 reshape.126
  277.6 20.6 %all-to-all-done.2 = f32[32,16,2]{1,2,0:T(2,128)} async-done(((f32[32,16,2]{1,2,0:T(2,128)}), f32[32,16,2]{1,2,0:T(2,128)}, u32[]{:S(2)}, u32[]{:S(2)}) %all-to-all-start.2) | async-done | bytes 4128 | tf_op jit(solution)/shard_map/all_to_all | solution.py:21
  298.2 1.5 fusion.23
  299.7 1.4 copy.131
  301.1 1.5 slice.91
  302.6 1.5 slice.92
  304.1 1.4 copy.134
  305.5 1.5 slice.102
  307.0 1.5 slice.103
  308.5 1.4 copy.136
  309.9 1.4 copy.135
  311.3 1.4 copy.133
  312.7 1.4 copy.132
  314.1 0.9 multiply_add_fusion
  315.0 0.7 dynamic-slice_reduce_fusion
  315.8 0.6 fusion.22
  316.5 0.7 copy.119
  317.1 0.8 divide_bitcast_fusion
  317.9 0.7 fusion.14
  318.6 1.2 fusion.6
  319.8 0.7 broadcast_in_dim.11
  320.5 5.4 %all-to-all-start.3 = ((f32[32,4,2,128]{3,2,1,0:T(2,128)}), f32[32,4,2,128]{3,2,1,0:T(2,128)}, u32[]{:S(2)}, u32[]{:S(2)}) async-start(f32[32,4,2,128]{3,2,1,0:T(2,128)} %broadcast_in_dim.11), calls=%async_computation.3 | async-start | bytes 262144 | tf_op jit(solution)/shard_map/all_to_all | solution.py:21
  325.9 0.7 reshape.127
  326.6 0.7 broadcast_bitcast_fusion.2
  327.2 0.8 bitcast_convert_fusion
  328.0 0.1 copy.122
  328.1 24.5 %all-to-all-done.3 = f32[32,4,2,128]{3,2,1,0:T(2,128)} async-done(((f32[32,4,2,128]{3,2,1,0:T(2,128)}), f32[32,4,2,128]{3,2,1,0:T(2,128)}, u32[]{:S(2)}, u32[]{:S(2)}) %all-to-all-start.3) | async-done | bytes 131104 | tf_op jit(solution)/shard_map/all_to_all | solution.py:21
  352.6 1.0 reduce_sum.43
  353.5 0.2 broadcast_bitcast_fusion.1
  353.8 1.3 fusion.12
  355.0 0.7 copy.184
  355.8 1.8 copy.185
  (21 shorter events, 0.5 us)
Async XLA Ops:
  7.2 166.6 %copy-start = (bf16[4,192,2048]{2,1,0:T(8,128)(2,1)S(1)}, bf16[4,192,2048]{2,1,0:T(8,128)(2,1)}, u32[]{:S(2)}) copy-start(bf16[4,192,2048]{2,1,0:T(8,128)(2,1)} %param.8) | copy-start | bytes 9437188
  7.2 166.6 %all-gather.2.cloned.1.call-start = ((), (), s32[]{:S(2)}) async-start(), calls=%async_computation.4 | async-start | bytes 2162688 | tf_op jit(solution)/shard_map/all_gather | solution.py:12
  177.0 48.9 %all-to-all-start = ((bf16[32,1,24,256]{3,2,1,0:T(8,128)(2,1)}), bf16[32,1,24,256]{3,2,1,0:T(8,128)(2,1)S(1)}, u32[]{:S(2)}, u32[]{:S(2)}) async-start(bf16[32,1,24,256]{3,2,1,0:T(8,128)(2,1)} %bitcast.90), calls=%async_computation | async-start | bytes 786432 | tf_op jit(solution)/shard_map/all_to_all | solution.py:153
  188.1 43.2 %copy-start.1 = (bf16[4,256]{1,0:T(4,128)(2,1)S(1)}, bf16[4,256]{1,0:T(4,128)(2,1)}, u32[]{:S(2)}) copy-start(bf16[4,256]{1,0:T(4,128)(2,1)} %param.11) | copy-start | bytes 6148
  188.1 43.8 %copy-start.2 = (bf16[4,256]{1,0:T(4,128)(2,1)S(1)}, bf16[4,256]{1,0:T(4,128)(2,1)}, u32[]{:S(2)}) copy-start(bf16[4,256]{1,0:T(4,128)(2,1)} %param.12) | copy-start | bytes 6148
  225.8 43.3 %all-to-all-start.1 = ((bf16[32,1,24,256]{3,2,1,0:T(8,128)(2,1)}), bf16[32,1,24,256]{3,2,1,0:T(8,128)(2,1)}, u32[]{:S(2)}, u32[]{:S(2)}) async-start(bf16[32,1,24,256]{3,2,1,0:T(8,128)(2,1)} %bitcast.89), calls=%async_computation.1 | async-start | bytes 786432 | tf_op jit(solution)/shard_map/all_to_all | solution.py:154
  270.4 27.7 %all-to-all-start.2 = ((f32[32,16,2]{1,2,0:T(2,128)}), f32[32,16,2]{1,2,0:T(2,128)}, u32[]{:S(2)}, u32[]{:S(2)}) async-start(f32[32,16,2]{1,2,0:T(2,128)} %broadcast_in_dim.9), calls=%async_computation.2 | async-start | bytes 65536 | tf_op jit(solution)/shard_map/all_to_all | solution.py:21
  320.5 32.1 %all-to-all-start.3 = ((f32[32,4,2,128]{3,2,1,0:T(2,128)}), f32[32,4,2,128]{3,2,1,0:T(2,128)}, u32[]{:S(2)}, u32[]{:S(2)}) async-start(f32[32,4,2,128]{3,2,1,0:T(2,128)} %broadcast_in_dim.11), calls=%async_computation.3 | async-start | bytes 262144 | tf_op jit(solution)/shard_map/all_to_all | solution.py:21
Sparse Core Ops, SparseCore 0:
  10.7 163.0 all-gather.1
where the time goes:
time: 366 us; the launch traced here: 364 us
  waiting for transfers between devices  260 us (71%)
  local copies, waits for them, and re-layouts  42 us (11%)
  starting transfers between devices  27.3 us (7%)
  between operations  14.2 us (4%)
  other arithmetic  13.2 us (4%)
  matrix products  7.87 us (2%)
    all_gather x1, waiting for transfers between devices, sent_together(): lax.all_gather(both, axis, axis=dim, tiled=True)  165 us
    all_to_all x2, waiting for transfers between devices, copy_for_each(): lax.all_to_all(jnp.broadcast_to(shard[None], (peers, *shard.shape)), axis...  45 us
    all_to_all x1, waiting for transfers between devices, body(): lax.all_to_all(key_blocks, 'sp', split_axis=0, concat_axis=1, tiled=True)  32.8 us
    all_to_all x1, waiting for transfers between devices, body(): lax.all_to_all(value_blocks, 'sp', split_axis=0, concat_axis=1, tiled=True)  17.1 us
    all_to_all x1, starting transfers between devices, body(): lax.all_to_all(key_blocks, 'sp', split_axis=0, concat_axis=1, tiled=True)  11.1 us
    unnamed x15, local copies, waits for them, and re-layouts  11 us
    all_to_all x2, starting transfers between devices, copy_for_each(): lax.all_to_all(jnp.broadcast_to(shard[None], (peers, *shard.shape)), axis...  10.7 us
  transfers between devices with their start and end apart: 5, of which 5 were waited for; matrix products, arithmetic and copies ran while one was open for 8% of the time, Pallas kernels for 0%

commit v1 on v0

--- a/solution.py
+++ b/solution.py
@@ -1,3 +1,4 @@
+import functools
 import jax
 import jax.numpy as jnp
 from jax import lax
@@ -5,6 +6,21 @@
 
 HALF = 64
 VDIM = 128
+
+
+def _replace_tracks(x_local, link_axis):
+    return jnp.concatenate(
+        lax.all_to_all(
+            jnp.stack(jnp.split(x_local, lax.axis_size(link_axis), axis=0), axis=0),
+            axis_name=link_axis,
+            split_axis=0,
+            concat_axis=0,
+        ),
+        axis=1,
+    )
+
+
+_clear_works = functools.partial(_replace_tracks, link_axis="sp")
 
 
 def sent_together(arrays, axis, dim, along):
@@ -150,7 +166,7 @@
     key_blocks = keys.reshape(count * spread, 1, sub, -1)
     value_blocks = values.reshape(count * spread, 1, sub, -1)
     key_cache, value_cache = (
-        lax.all_to_all(key_blocks, "sp", split_axis=0, concat_axis=1, tiled=True),
+        _clear_works(key_blocks),
         lax.all_to_all(value_blocks, "sp", split_axis=0, concat_axis=1, tiled=True),
     )
     first_read = block_read(

time: 366 us -> 446 us (1.22)
  local copies, waits for them, and re-layouts: 42 us -> 120 us
    another operation x5 -> x40, local copies, waits for them, and re-layouts: 4.9 us -> 47.2 us  [the longest x35 42.3 us: _replace_tracks(): jnp.stack(jnp.split(x_local, lax.axis_size(link_axis), axis=0), axis=0)]
    unnamed x15 -> x46, local copies, waits for them, and re-layouts: 11 us -> 47.4 us
  transfers between devices with their start and end apart: 5 -> 5, of which waited for: 5 -> 5; matrix products, arithmetic and copies ran while one was open for 8% -> 7% of each run, Pallas kernels for 0% -> 0%
where the time goes in v1:
time: 446 us; the launch traced here: 442 us
  waiting for transfers between devices  258 us (58%)
  local copies, waits for them, and re-layouts  120 us (27%)
  starting transfers between devices  29.2 us (7%)
  between operations  14.3 us (3%)
  other arithmetic  13.2 us (3%)
  matrix products  7.87 us (2%)
    all_gather x1, waiting for transfers between devices, sent_together(): lax.all_gather(both, axis, axis=dim, tiled=True)  163 us
    unnamed x46, local copies, waits for them, and re-layouts  47.4 us
    all_to_all x2, waiting for transfers between devices, copy_for_each(): lax.all_to_all(jnp.broadcast_to(shard[None], (peers, *shard.shape)), axis...  45 us
    another operation x35, local copies, waits for them, and re-layouts, _replace_tracks(): jnp.stack(jnp.split(x_local, lax.axis_size(link_axis), axis=0), axis=0)  42.3 us
    all_to_all x1, waiting for transfers between devices, _replace_tracks(): lax.all_to_all(jnp.stack(jnp.split(x_local, lax.axis_size(link_axis), axi...  32.8 us
    all_to_all x1, waiting for transfers between devices, body(): lax.all_to_all(value_blocks, 'sp', split_axis=0, concat_axis=1, tiled=True)  17.1 us
    all_to_all x1, starting transfers between devices, _replace_tracks(): lax.all_to_all(jnp.stack(jnp.split(x_local, lax.axis_size(link_axis), axi...  12.9 us
    all_to_all x2, starting transfers between devices, copy_for_each(): lax.all_to_all(jnp.broadcast_to(shard[None], (peers, *shard.shape)), axis...  10.8 us
  transfers between devices with their start and end apart: 5, of which 5 were waited for; matrix products, arithmetic and copies ran while one was open for 7% of the time, Pallas kernels for 0%

profile of v1, /device:TPU:34, one launch (start us, length us, event | category | flops | bytes accessed | tf_op | source)
XLA Modules:
  0.0 442.1 jit_solution(13016711477766787242)
XLA Ops:
  7.3 1.6 pad_maximum_fusion
  8.9 163.1 %all-gather.2.cloned.1.call-done = bf16[2048,512]{1,0:T(8,128)(2,1)} async-done(((bf16[64,512]{1,0:T(8,128)(2,1)}), bf16[2048,512]{1,0:T(8,128)(2,1)}) %all-gather.2.cloned.1.call-update) | async-done | bytes 2097168 | tf_op jit(solution)/shard_map/all_gather | solution.py:28
  172.0 2.2 fusion
  175.4 1.3 slice_bitcast_fusion
  176.7 1.5 copy.235
  178.2 1.5 copy.234
  179.7 1.5 copy.233
  181.2 1.5 copy.232
  182.7 1.5 copy.231
  184.3 1.5 copy.230
  185.8 1.5 copy.229
  187.3 1.5 copy.228
  188.8 1.5 copy.227
  190.3 1.5 copy.226
  191.8 1.5 copy.225
  193.3 1.5 copy.224
  197.3 1.5 copy.253
  198.8 1.5 copy.252
  200.3 1.5 copy.251
  201.8 1.5 copy.250
  203.3 1.5 copy.249
  204.9 1.5 copy.248
  206.4 1.5 copy.247
  207.9 1.5 copy.246
  209.4 1.5 copy.245
  210.9 1.5 copy.244
  212.4 1.5 copy.243
  213.9 1.5 copy.242
  216.5 1.3 constant_dynamic-update-slice_fusion.30
  217.9 1.3 constant_dynamic-update-slice_fusion.29
  219.2 1.3 constant_dynamic-update-slice_fusion.28
  252.8 12.9 %all-to-all-start = ((bf16[32,1,1,24,256]{4,3,2,1,0:T(8,128)(2,1)}), bf16[32,1,1,24,256]{4,3,2,1,0:T(8,128)(2,1)S(1)}, u32[]{:S(2)}, u32[]{:S(2)}) async-start(bf16[32,1,1,24,256]{4,3,2,1,0:T(8,128)(2,1)} %constant_dynamic-update-slice_fusion), calls=%async_computation | async-start | bytes 786432 | tf_op jit(solution)/shard_map/all_to_all | solution.py:13
  265.8 3.0 fusion.1
  268.8 1.9 copy.255
  270.7 32.8 %all-to-all-done = bf16[32,1,1,24,256]{4,3,2,1,0:T(8,128)(2,1)S(1)} async-done(((bf16[32,1,1,24,256]{4,3,2,1,0:T(8,128)(2,1)}), bf16[32,1,1,24,256]{4,3,2,1,0:T(8,128)(2,1)S(1)}, u32[]{:S(2)}, u32[]{:S(2)}) %all-to-all-start) | async-done | bytes 393248 | tf_op jit(solution)/shard_map/all_to_all | solution.py:13
  303.5 5.4 %all-to-all-start.1 = ((bf16[32,1,24,256]{3,2,1,0:T(8,128)(2,1)}), bf16[32,1,24,256]{3,2,1,0:T(8,128)(2,1)}, u32[]{:S(2)}, u32[]{:S(2)}) async-start(bf16[32,1,24,256]{3,2,1,0:T(8,128)(2,1)} %bitcast.150), calls=%async_computation.1 | async-start | bytes 786432 | tf_op jit(solution)/shard_map/all_to_all | solution.py:170
  311.7 1.5 fusion.4
  313.9 1.3 copy.258
  315.2 1.3 dynamic-slice_maximum_fusion
  316.6 1.3 copy.260
  317.9 1.3 copy.259
  321.1 1.3 reshape.185
  322.4 1.4 exponential_reduce_fusion
  323.8 1.3 copy.261
  327.0 1.3 reshape.186
  328.4 1.3 pad_maximum_fusion.1
  329.7 17.1 %all-to-all-done.1 = bf16[32,1,24,256]{3,2,1,0:T(8,128)(2,1)} async-done(((bf16[32,1,24,256]{3,2,1,0:T(8,128)(2,1)}), bf16[32,1,24,256]{3,2,1,0:T(8,128)(2,1)}, u32[]{:S(2)}, u32[]{:S(2)}) %all-to-all-start.1) | async-done | bytes 393248 | tf_op jit(solution)/shard_map/all_to_all | solution.py:170
  348.1 5.4 %all-to-all-start.2 = ((f32[32,16,2]{1,2,0:T(2,128)}), f32[32,16,2]{1,2,0:T(2,128)}, u32[]{:S(2)}, u32[]{:S(2)}) async-start(f32[32,16,2]{1,2,0:T(2,128)} %broadcast_in_dim.9), calls=%async_computation.2 | async-start | bytes 65536 | tf_op jit(solution)/shard_map/all_to_all | solution.py:37
  353.5 1.8 reshape.187
  355.3 20.6 %all-to-all-done.2 = f32[32,16,2]{1,2,0:T(2,128)} async-done(((f32[32,16,2]{1,2,0:T(2,128)}), f32[32,16,2]{1,2,0:T(2,128)}, u32[]{:S(2)}, u32[]{:S(2)}) %all-to-all-start.2) | async-done | bytes 4128 | tf_op jit(solution)/shard_map/all_to_all | solution.py:37
  375.9 1.5 fusion.23
  377.4 1.4 copy.282
  378.9 1.5 slice.123
  380.3 1.5 slice.124
  381.8 1.4 copy.285
  383.2 1.5 slice.134
  384.7 1.5 slice.135
  386.2 1.4 copy.287
  387.6 1.4 copy.286
  389.0 1.4 copy.284
  390.4 1.4 copy.283
  398.2 5.4 %all-to-all-start.3 = ((f32[32,4,2,128]{3,2,1,0:T(2,128)}), f32[32,4,2,128]{3,2,1,0:T(2,128)}, u32[]{:S(2)}, u32[]{:S(2)}) async-start(f32[32,4,2,128]{3,2,1,0:T(2,128)} %broadcast_in_dim.11), calls=%async_computation.3 | async-start | bytes 262144 | tf_op jit(solution)/shard_map/all_to_all | solution.py:37
  405.8 24.5 %all-to-all-done.3 = f32[32,4,2,128]{3,2,1,0:T(2,128)} async-done(((f32[32,4,2,128]{3,2,1,0:T(2,128)}), f32[32,4,2,128]{3,2,1,0:T(2,128)}, u32[]{:S(2)}, u32[]{:S(2)}) %all-to-all-start.3) | async-done | bytes 131104 | tf_op jit(solution)/shard_map/all_to_all | solution.py:37
  433.5 1.8 copy.367
  (86 shorter events, 57.4 us)
Async XLA Ops:
  7.2 164.8 %copy-start = (bf16[4,192,2048]{2,1,0:T(8,128)(2,1)S(1)}, bf16[4,192,2048]{2,1,0:T(8,128)(2,1)}, u32[]{:S(2)}) copy-start(bf16[4,192,2048]{2,1,0:T(8,128)(2,1)} %param.8) | copy-start | bytes 9437188
  7.2 164.8 %all-gather.2.cloned.1.call-start = ((), (), s32[]{:S(2)}) async-start(), calls=%async_computation.4 | async-start | bytes 2162688 | tf_op jit(solution)/shard_map/all_gather | solution.py:28
  252.8 50.7 %all-to-all-start = ((bf16[32,1,1,24,256]{4,3,2,1,0:T(8,128)(2,1)}), bf16[32,1,1,24,256]{4,3,2,1,0:T(8,128)(2,1)S(1)}, u32[]{:S(2)}, u32[]{:S(2)}) async-start(bf16[32,1,1,24,256]{4,3,2,1,0:T(8,128)(2,1)} %constant_dynamic-update-slice_fusion), calls=%async_computation | async-start | bytes 786432 | tf_op jit(solution)/shard_map/all_to_all | solution.py:13
  265.8 43.2 %copy-start.1 = (bf16[4,256]{1,0:T(4,128)(2,1)S(1)}, bf16[4,256]{1,0:T(4,128)(2,1)}, u32[]{:S(2)}) copy-start(bf16[4,256]{1,0:T(4,128)(2,1)} %param.11) | copy-start | bytes 6148
  265.8 43.9 %copy-start.2 = (bf16[4,256]{1,0:T(4,128)(2,1)S(1)}, bf16[4,256]{1,0:T(4,128)(2,1)}, u32[]{:S(2)}) copy-start(bf16[4,256]{1,0:T(4,128)(2,1)} %param.12) | copy-start | bytes 6148
  303.5 43.3 %all-to-all-start.1 = ((bf16[32,1,24,256]{3,2,1,0:T(8,128)(2,1)}), bf16[32,1,24,256]{3,2,1,0:T(8,128)(2,1)}, u32[]{:S(2)}, u32[]{:S(2)}) async-start(bf16[32,1,24,256]{3,2,1,0:T(8,128)(2,1)} %bitcast.150), calls=%async_computation.1 | async-start | bytes 786432 | tf_op jit(solution)/shard_map/all_to_all | solution.py:170
  348.1 27.8 %all-to-all-start.2 = ((f32[32,16,2]{1,2,0:T(2,128)}), f32[32,16,2]{1,2,0:T(2,128)}, u32[]{:S(2)}, u32[]{:S(2)}) async-start(f32[32,16,2]{1,2,0:T(2,128)} %broadcast_in_dim.9), calls=%async_computation.2 | async-start | bytes 65536 | tf_op jit(solution)/shard_map/all_to_all | solution.py:37
  398.2 32.1 %all-to-all-start.3 = ((f32[32,4,2,128]{3,2,1,0:T(2,128)}), f32[32,4,2,128]{3,2,1,0:T(2,128)}, u32[]{:S(2)}, u32[]{:S(2)}) async-start(f32[32,4,2,128]{3,2,1,0:T(2,128)} %broadcast_in_dim.11), calls=%async_computation.3 | async-start | bytes 262144 | tf_op jit(solution)/shard_map/all_to_all | solution.py:37
Sparse Core Ops, SparseCore 0:
  10.7 161.2 all-gather.1
